TPU v7x, 32 devices: a whole 2x2x4 slice. The times are simulated.
32 devices in a mesh: gr: 2 (over x), sp: 8 (over z, y), tp: 2 (over core).
Axes of the slice: x: 2, y: 2, z: 4, core: 2. Of those that a mesh axis runs over, the one named last changes fastest.
Arguments:
- tokens: bfloat16 [8, 1536, 2048], P('gr', 'sp'), parts along dimension 0, may hold values from -6 to 6
- key_weight: bfloat16 [2048, 512], P(None, 'tp'), may hold values from -0.125 to 0.125
- value_weight: bfloat16 [2048, 1024], P(None, 'tp'), may hold values from -0.125 to 0.125
- input_weight: bfloat16 [2048, 8], P(None, 'tp'), may hold values from -0.125 to 0.125
- forget_weight: bfloat16 [2048, 8], P(None, 'tp'), may hold values from -0.125 to 0.125
- forget_bias: float32 [8], P('tp'), may hold values from 2.5 to 9.5
- query: bfloat16 [8, 512], P('gr', 'tp'), parts along dimension 0, may hold values from -6 to 6
Outputs:
- key_cache: bfloat16 [16, 768, 512], P(('gr', 'sp'), None, 'tp'), parts along dimension 0
- value_cache: bfloat16 [16, 768, 1024], P(('gr', 'sp'), None, 'tp'), parts along dimension 0
- memory: float32 [8, 8, 64, 128], P('gr', 'tp'), parts along dimension 0
- normalizer: float32 [8, 8, 64], P('gr', 'tp'), parts along dimension 0
- stabilizer: float32 [8, 8], P('gr', 'tp'), parts along dimension 0
- first_read: float32 [8, 1024], P('gr', 'tp'), parts along dimension 0
There are 2 independent parts, one for each index of `gr`. A program takes and returns all parts, laid end to end along the dimension named above; an argument that names none is the same for every part. Nothing has to cross between parts.
All inputs are finite; a program needn't handle non-finite values.
Results may differ from a plain program's by a relative error of at most 0.0015.
The roundings to bfloat16 on the way count: a program that leaves them out, or rounds other values in their place, can miss the bound.
Values may be sent and summed in bfloat16 or wider, within the bound.
A program may use at most 64 MiB of HBM per device.

v0:
```python
import jax
import jax.numpy as jnp
from jax import lax
from jax.sharding import PartitionSpec as P


def carried_in(array, axis, combine, identity):
    size, index = (lax.axis_size(axis), lax.axis_index(axis))
    everything = lax.all_gather(array, axis)
    start = jnp.broadcast_to(jnp.asarray(identity, array.dtype), array.shape)

    def step(k, before):
        at = size - 1 - k
        reached = at > index
        new = combine(before, everything[at])
        return jnp.where(reached, new, before)

    return lax.fori_loop(0, size, step, start)


def merged(value, axis, join):
    pieces = jax.tree.map(lambda part: lax.all_gather(part, axis), value)
    head = jax.tree.map(lambda part: part[0], pieces)
    tail = jax.tree.map(lambda part: part[1:], pieces)
    so_far, _ = lax.scan(lambda so_far, share: (join(so_far, share), None), head, tail)
    return so_far


def add_pair(earlier, later):
    return earlier + later


def block_state(keys3, values3, igate, logf, later, kdim):
    seqs, span, heads = logf.shape
    total = jnp.sum(logf, axis=1)
    logw = (later + total)[:, None, :] - jnp.cumsum(logf, axis=1) + igate
    top = jnp.max(logw, axis=1)
    weight = jnp.exp(logw - top[:, None, :]) * kdim ** (-0.5)
    keys4 = keys3.reshape(seqs, span, heads, kdim).astype(jnp.float32)
    values4 = values3.reshape(seqs, span, heads, -1).astype(jnp.float32)
    scaled = keys4 * weight[..., None]
    memory = jnp.einsum("slhd,slhe->shde", scaled, values4, precision=lax.Precision.HIGHEST)
    return (memory, jnp.sum(scaled, axis=1), top, total)


def merge_states(first, second):
    top = jnp.maximum(first[2], second[2])
    left = jnp.exp(first[2] - top)
    right = jnp.exp(second[2] - top)
    memory = first[0] * left[..., None, None] + second[0] * right[..., None, None]
    normal = first[1] * left[..., None] + second[1] * right[..., None]
    return (memory, normal, top, first[3] + second[3])


def local(tokens, key_weight, value_weight, input_weight, forget_weight, forget_bias, query):
    seqs, span, width = tokens.shape
    heads = input_weight.shape[1]
    kdim = key_weight.shape[1] // heads
    vdim = value_weight.shape[1] // heads
    pieces = lax.axis_size("sp") // seqs
    sub = span // pieces
    flat = tokens.reshape(seqs * span, width)
    keys = jnp.dot(flat, key_weight, preferred_element_type=jnp.float32).astype(jnp.bfloat16)
    values = jnp.dot(flat, value_weight, preferred_element_type=jnp.float32).astype(jnp.bfloat16)
    gate_pair = jnp.concatenate([input_weight, forget_weight], axis=1)
    gates = jnp.dot(flat, gate_pair, preferred_element_type=jnp.float32)
    igate = gates[:, :heads].reshape(seqs, span, heads)
    logf = jax.nn.log_sigmoid(gates[:, heads:] + forget_bias).reshape(seqs, span, heads)
    keys3 = keys.reshape(seqs, span, heads * kdim)
    values3 = values.reshape(seqs, span, heads * vdim)
    key_cache, value_cache = (
        lax.all_to_all(
            keys3.reshape(seqs * pieces, sub, heads * kdim),
            "sp",
            split_axis=0,
            concat_axis=1,
            tiled=True,
        ),
        lax.all_to_all(
            values3.reshape(seqs * pieces, sub, heads * vdim),
            "sp",
            split_axis=0,
            concat_axis=1,
            tiled=True,
        ),
    )
    zeros = jnp.zeros((seqs, heads), jnp.float32)
    later = carried_in(jnp.sum(logf, axis=1), "sp", add_pair, zeros)
    memory_part, normal_part, top, total = block_state(keys3, values3, igate, logf, later, kdim)
    memory_all, normal_all, top_all, total_all = merged(
        (memory_part, normal_part, top, total), "sp", merge_states
    )
    stabilizer = jnp.maximum(top_all, total_all)
    factor = jnp.exp(top_all - stabilizer)
    memory = memory_all * factor[..., None, None]
    normalizer = normal_all * factor[..., None]
    asked = query.astype(jnp.float32).reshape(query.shape[0], heads, kdim)
    numer = jnp.einsum("shd,shde->she", asked, memory, precision=lax.Precision.HIGHEST)
    denom = jnp.maximum(jnp.abs(jnp.sum(asked * normalizer, axis=-1)), 1.0)
    first_read = (numer / denom[..., None]).reshape(query.shape[0], heads * vdim)
    return (key_cache, value_cache, memory, normalizer, stabilizer, first_read)


def solution(mesh):
    return jax.shard_map(
        local,
        mesh=mesh,
        in_specs=(
            P("gr", "sp", None),
            P(None, "tp"),
            P(None, "tp"),
            P(None, "tp"),
            P(None, "tp"),
            P("tp"),
            P("gr", "tp"),
        ),
        out_specs=(
            P(("gr", "sp"), None, "tp"),
            P(("gr", "sp"), None, "tp"),
            P("gr", "tp", None, None),
            P("gr", "tp", None),
            P("gr", "tp"),
            P("gr", "tp"),
        ),
        check_vma=False,
    )
```

profile of v0, /device:TPU:0, one launch (start us, length us, event | category | flops | bytes accessed | tf_op | source)
XLA Modules:
  0.0 211.6 jit_solution(7671632423110484531)
XLA Ops:
  7.2 1.8 copy-done
  9.1 2.4 %convolution_convert_fusion.1 = bf16[768,256]{1,0:T(8,128)(2,1)S(1)} fusion(bf16[768,2048]{1,0:T(8,128)(2,1)S(1)} %bitcast.70, bf16[2048,256]{1,0:T(8,128)(2,1)} %param.12), kind=kOutput, calls=%fused_computation.11 | convolution fusion | flops 805502976 | bytes 4587520 | tf_op jit(solution)/shard_map/dot_general | solution.py:63
  11.4 2.7 %convolution_convert_fusion = bf16[768,512]{1,0:T(8,128)(2,1)} fusion(bf16[768,2048]{1,0:T(8,128)(2,1)S(1)} %bitcast.71, bf16[2048,512]{1,0:T(8,128)(2,1)S(1)} %copy-done.6), kind=kOutput, calls=%fused_computation.10 | convolution fusion | flops 1611005952 | bytes 6029312 | tf_op jit(solution)/shard_map/dot_general | solution.py:64
  14.1 1.1 copy.31
  15.2 2.8 %reshape.70 = f32[4,192,4,64]{1,0,3,2:T(4,128)} reshape(f32[768,256]{0,1:T(8,128)} %copy.31) | data formatting | bytes 1572864 | tf_op jit(solution)/shard_map/convert_element_type | solution.py:39
  18.1 1.6 convolution_bitcast_fusion
  20.1 4.8 %reduce-window.6 = f32[4,4,2,128]{3,2,1,0:T(2,128)S(1)} reduce-window(f32[4,4,2,128]{3,2,1,0:T(2,128)S(1)} %copy.34, f32[]{:T(128)} %constant.71.clone.1), window={size=1x1x1x128 pad=0_0x0_0x0_0x127_0}, to_apply=%region_3.4 | reduce-window | flops 520192 | bytes 32772 | tf_op jit(solution)/shard_map/reduce-window
  25.1 0.1 copy.35
  25.2 0.1 copy.36
  25.6 27.9 %all-gather.4 = f32[8,4,4]{2,1,0:T(4,128)S(1)} all-gather(f32[1,4,4]{2,1,0:T(4,128)S(1)} %bitcast.83), channel_id=2, replica_groups=mesh['gr'=2,'sp'=8,'tp'=2] {'sp'}, dimensions={0}, use_global_device_ids=true | all-gather | bytes 576 | tf_op jit(solution)/shard_map/all_gather | solution.py:9
  53.5 0.3 while.33
  53.9 0.2 fusion.14
  54.2 2.4 %reshape_reshape.12 = bf16[4,192,4,128]{3,2,1,0:T(4,128)(2,1)} reshape(bf16[768,512]{1,0:T(8,128)(2,1)} %convolution_convert_fusion) | data formatting | bytes 1572864 | tf_op jit(solution)/shard_map/reshape;reshape | solution.py:40
  56.6 2.3 %fusion.16 = (f32[4,4,64]{0,2,1:T(8,128)}, f32[4,192,4,64]{1,0,3,2:T(4,128)S(1)}) fusion(f32[4,192,4,64]{1,0,3,2:T(4,128)} %reshape.70, f32[4,192,4]{1,0,2:T(4,128)S(1)} %exponential_multiply_fusion), kind=kLoop, calls=%fused_computation.42 | loop fusion | flops 392192 | bytes 1589248 | tf_op jit(solution)/shard_map/reduce_sum | solution.py:43
  58.9 2.9 %fusion.3 = f32[4,4,64,128]{3,2,1,0:T(8,128)} fusion(f32[4,192,4,64]{1,0,3,2:T(4,128)S(1)} %get-tuple-element.219, bf16[4,192,4,128]{3,2,1,0:T(4,128)(2,1)} %reshape_reshape.12), kind=kOutput, calls=%fused_computation.13 | convolution fusion | flops 301989888 | bytes 2097152 | tf_op jit(solution)/shard_map/slhd,slhe->shde/dot_general | solution.py:42
  61.8 15.3 %all_to_all.24 = bf16[8,96,256]{2,1,0:T(8,128)(2,1)S(1)} all-to-all(bf16[8,96,256]{2,1,0:T(8,128)(2,1)} %bitcast.76), channel_id=1, replica_groups=mesh['gr'=2,'sp'=8,'tp'=2] {'sp'}, dimensions={0} | all-to-all | bytes 786432 | tf_op jit(solution)/shard_map/all_to_all | solution.py:72
  77.2 10.2 %all-to-all-start.1 = ((bf16[8,96,512]{2,1,0:T(8,128)(2,1)}), bf16[8,96,512]{2,1,0:T(8,128)(2,1)}, u32[]{:S(2)}, u32[]{:S(2)}) async-start(bf16[8,96,512]{2,1,0:T(8,128)(2,1)} %bitcast.74), calls=%async_computation.1 | async-start | bytes 1572864 | tf_op jit(solution)/shard_map/all_to_all | solution.py:79
  87.4 1.0 copy.40
  88.4 41.4 %all-gather.2 = f32[32,4,64]{2,1,0:T(4,128)S(1)} all-gather(f32[4,4,64]{2,1,0:T(4,128)S(1)} %copy.40), channel_id=4, replica_groups=mesh['gr'=2,'sp'=8,'tp'=2] {'sp'}, dimensions={0}, use_global_device_ids=true | all-gather | bytes 36864 | tf_op jit(solution)/shard_map/all_gather | solution.py:22
  129.8 0.6 slice.75
  130.4 1.3 slice.76
  131.7 0.7 reshape.67
  132.4 0.7 reshape.101
  133.1 26.5 %all-gather.5 = f32[8,4,4]{2,1,0:T(4,128)S(1)} all-gather(f32[1,4,4]{2,1,0:T(4,128)S(1)} %bitcast.82), channel_id=5, replica_groups=mesh['gr'=2,'sp'=8,'tp'=2] {'sp'}, dimensions={0}, use_global_device_ids=true | all-gather | bytes 576 | tf_op jit(solution)/shard_map/all_gather | solution.py:22
  159.6 0.6 slice.73
  160.2 0.7 slice_bitcast_fusion
  160.9 1.9 slice.69
  162.8 4.4 %slice.74 = f32[28,4,64,128]{3,2,1,0:T(8,128)} slice(f32[32,4,64,128]{3,2,1,0:T(8,128)} %all-gather.8.cloned.1.call-done), slice={[4:32], [0:4], [0:64], [0:128]} | slice | bytes 7340032 | tf_op jit(solution)/shard_map/slice | solution.py:24
  167.1 30.0 %while.32 = (s32[]{:T(128)}, f32[4,4,64,128]{3,2,1,0:T(8,128)}, f32[4,4,64]{2,1,0:T(4,128)S(1)}, f32[4,4]{1,0:T(4,128)S(1)}, f32[4,4]{1,0:T(4,128)S(1)}, /*index...) while((s32[]{:T(128)}, f32[4,4,64,128]{3,2,1,0:T(8,128)}, ...), condition=%wide.region_8.9_spmd, body=%wide.region_7.8_spmd.sunk | while | flops 396354 | bytes 1586173 | solution.py:25
  167.1 0.7 subtract_exponential_fusion.3
  167.8 0.7 bitcast_add_fusion.2
  168.5 2.1 %fusion.27 = f32[4,4,64,128]{3,2,1,0:T(8,128)} fusion(f32[7,4,4,64,128]{4,3,2,1,0:T(8,128)} %get-tuple-element.362, s32[]{:T(128)S(6)} %copy.64, f32[4,4,64,128]{3,2,1,0:T(8,128)} %get-tuple-element.347, f32[4,4]{1,0:T(4,128)S(1)} %get-tuple-element.305, f32[4,4]{1,0:T(4,128)S(1)} %get-tuple-element.306), kind=kLoop, calls=%fused_computation.1.clone.1 | loop fusion | flops 393216 | bytes 1572996 | tf_op jit(solution)/shard_map/while/body/eval_jaxpr/add | solution.py:50
  170.6 0.8 fusion.28
  171.4 0.7 subtract_exponential_fusion.3
  172.1 0.7 bitcast_add_fusion.2
  172.8 2.1 %fusion.27 = f32[4,4,64,128]{3,2,1,0:T(8,128)} fusion(f32[7,4,4,64,128]{4,3,2,1,0:T(8,128)} %get-tuple-element.362, s32[]{:T(128)S(6)} %copy.64, f32[4,4,64,128]{3,2,1,0:T(8,128)} %get-tuple-element.347, f32[4,4]{1,0:T(4,128)S(1)} %get-tuple-element.305, f32[4,4]{1,0:T(4,128)S(1)} %get-tuple-element.306), kind=kLoop, calls=%fused_computation.1.clone.1 | loop fusion | flops 393216 | bytes 1572996 | tf_op jit(solution)/shard_map/while/body/eval_jaxpr/add | solution.py:50
  174.9 0.8 fusion.28
  175.7 0.7 subtract_exponential_fusion.3
  176.4 0.7 bitcast_add_fusion.2
  177.1 2.1 %fusion.27 = f32[4,4,64,128]{3,2,1,0:T(8,128)} fusion(f32[7,4,4,64,128]{4,3,2,1,0:T(8,128)} %get-tuple-element.362, s32[]{:T(128)S(6)} %copy.64, f32[4,4,64,128]{3,2,1,0:T(8,128)} %get-tuple-element.347, f32[4,4]{1,0:T(4,128)S(1)} %get-tuple-element.305, f32[4,4]{1,0:T(4,128)S(1)} %get-tuple-element.306), kind=kLoop, calls=%fused_computation.1.clone.1 | loop fusion | flops 393216 | bytes 1572996 | tf_op jit(solution)/shard_map/while/body/eval_jaxpr/add | solution.py:50
  179.2 0.8 fusion.28
  180.0 0.7 subtract_exponential_fusion.3
  180.7 0.7 bitcast_add_fusion.2
  181.4 2.1 %fusion.27 = f32[4,4,64,128]{3,2,1,0:T(8,128)} fusion(f32[7,4,4,64,128]{4,3,2,1,0:T(8,128)} %get-tuple-element.362, s32[]{:T(128)S(6)} %copy.64, f32[4,4,64,128]{3,2,1,0:T(8,128)} %get-tuple-element.347, f32[4,4]{1,0:T(4,128)S(1)} %get-tuple-element.305, f32[4,4]{1,0:T(4,128)S(1)} %get-tuple-element.306), kind=kLoop, calls=%fused_computation.1.clone.1 | loop fusion | flops 393216 | bytes 1572996 | tf_op jit(solution)/shard_map/while/body/eval_jaxpr/add | solution.py:50
  183.5 0.8 fusion.28
  184.3 0.7 subtract_exponential_fusion.3
  185.0 0.7 bitcast_add_fusion.2
  185.7 2.1 %fusion.27 = f32[4,4,64,128]{3,2,1,0:T(8,128)} fusion(f32[7,4,4,64,128]{4,3,2,1,0:T(8,128)} %get-tuple-element.362, s32[]{:T(128)S(6)} %copy.64, f32[4,4,64,128]{3,2,1,0:T(8,128)} %get-tuple-element.347, f32[4,4]{1,0:T(4,128)S(1)} %get-tuple-element.305, f32[4,4]{1,0:T(4,128)S(1)} %get-tuple-element.306), kind=kLoop, calls=%fused_computation.1.clone.1 | loop fusion | flops 393216 | bytes 1572996 | tf_op jit(solution)/shard_map/while/body/eval_jaxpr/add | solution.py:50
  187.8 0.8 fusion.28
  188.6 0.7 subtract_exponential_fusion.3
  189.3 0.7 bitcast_add_fusion.2
  189.9 2.1 %fusion.27 = f32[4,4,64,128]{3,2,1,0:T(8,128)} fusion(f32[7,4,4,64,128]{4,3,2,1,0:T(8,128)} %get-tuple-element.362, s32[]{:T(128)S(6)} %copy.64, f32[4,4,64,128]{3,2,1,0:T(8,128)} %get-tuple-element.347, f32[4,4]{1,0:T(4,128)S(1)} %get-tuple-element.305, f32[4,4]{1,0:T(4,128)S(1)} %get-tuple-element.306), kind=kLoop, calls=%fused_computation.1.clone.1 | loop fusion | flops 393216 | bytes 1572996 | tf_op jit(solution)/shard_map/while/body/eval_jaxpr/add | solution.py:50
  192.1 0.8 fusion.28
  192.8 0.7 subtract_exponential_fusion.3
  193.5 0.7 bitcast_add_fusion.2
  194.2 2.1 %fusion.27 = f32[4,4,64,128]{3,2,1,0:T(8,128)} fusion(f32[7,4,4,64,128]{4,3,2,1,0:T(8,128)} %get-tuple-element.362, s32[]{:T(128)S(6)} %copy.64, f32[4,4,64,128]{3,2,1,0:T(8,128)} %get-tuple-element.347, f32[4,4]{1,0:T(4,128)S(1)} %get-tuple-element.305, f32[4,4]{1,0:T(4,128)S(1)} %get-tuple-element.306), kind=kLoop, calls=%fused_computation.1.clone.1 | loop fusion | flops 393216 | bytes 1572996 | tf_op jit(solution)/shard_map/while/body/eval_jaxpr/add | solution.py:50
  196.3 0.8 fusion.28
  197.1 0.6 subtract_exponential_fusion.1
  197.7 1.1 broadcast_multiply_fusion.1
  198.9 1.3 multiply_reduce_fusion
  200.2 1.0 fusion.17
  201.4 0.6 copy.52
  202.0 0.7 copy.78
  202.7 2.1 copy.79
  (48 shorter events, 1.3 us)
Async XLA Ops:
  7.2 1.9 copy-start
  7.2 153.7 %all-gather.8.cloned.1.call-start = ((), (), s32[]{:S(2)}) async-start(), calls=%async_computation.2 | async-start | bytes 4718592 | tf_op jit(solution)/shard_map/all_gather | solution.py:22
  9.1 2.4 %copy-start.6 = (bf16[2048,512]{1,0:T(8,128)(2,1)S(1)}, bf16[2048,512]{1,0:T(8,128)(2,1)}, u32[]{:S(2)}) copy-start(bf16[2048,512]{1,0:T(8,128)(2,1)} %param.13) | copy-start | bytes 6291460
  11.4 2.7 %copy-start.2 = (bf16[768,256]{1,0:T(8,128)(2,1)}, bf16[768,256]{1,0:T(8,128)(2,1)S(1)}, u32[]{:S(2)}) copy-start(bf16[768,256]{1,0:T(8,128)(2,1)S(1)} %convolution_convert_fusion.1) | copy-start | bytes 1179652
  14.1 5.6 %copy-start.5 = (f32[4]{0:T(128)S(1)}, f32[4]{0:T(128)}, u32[]{:S(2)}) copy-start(f32[4]{0:T(128)} %param.16) | copy-start | bytes 52
  53.8 8.0 %copy-start.3 = (f32[8,4,4]{2,1,0:T(4,128)}, f32[8,4,4]{2,1,0:T(4,128)S(1)}, u32[]{:S(2)}) copy-start(f32[8,4,4]{2,1,0:T(4,128)S(1)} %get-tuple-element.384) | copy-start | bytes 1540
  58.9 72.8 %copy-start.4 = (bf16[4,256]{1,0:T(4,128)(2,1)S(1)}, bf16[4,256]{1,0:T(4,128)(2,1)}, u32[]{:S(2)}) copy-start(bf16[4,256]{1,0:T(4,128)(2,1)} %param.17) | copy-start | bytes 6148
  77.2 83.7 %all-to-all-start.1 = ((bf16[8,96,512]{2,1,0:T(8,128)(2,1)}), bf16[8,96,512]{2,1,0:T(8,128)(2,1)}, u32[]{:S(2)}, u32[]{:S(2)}) async-start(bf16[8,96,512]{2,1,0:T(8,128)(2,1)} %bitcast.74), calls=%async_computation.1 | async-start | bytes 1572864 | tf_op jit(solution)/shard_map/all_to_all | solution.py:79
  198.9 5.9 %copy-start.1 = (f32[4,4,64,128]{3,2,1,0:T(8,128)}, f32[4,4,64,128]{3,2,1,0:T(8,128)S(1)}, u32[]{:S(2)}) copy-start(f32[4,4,64,128]{3,2,1,0:T(8,128)S(1)} %broadcast_multiply_fusion.1) | copy-start | bytes 1572868
Sparse Core Ops, SparseCore 0:
  61.9 87.9 all-gather.7
where the time goes:
time: 213 us; the launch traced here: 212 us
  blocking collectives  111 us (52%)
  other arithmetic  40.9 us (19%)
  local copies, waits for them, and re-layouts  24.3 us (11%)
  between operations  14.2 us (7%)
  matrix products  10.6 us (5%)
  starting transfers between devices  10.2 us (5%)
    all_gather x2, blocking collectives, merged(): pieces = jax.tree.map(lambda part: lax.all_gather(part, axis), value)  67.9 us
    all_gather x1, blocking collectives, carried_in(): everything = lax.all_gather(array, axis)  27.9 us
    all_to_all x1, blocking collectives, local(): lax.all_to_all(keys3.reshape(seqs * pieces, sub, heads * kdim), 'sp', spl...  15.3 us
    add x7, other arithmetic, merge_states(): first[0] * left[..., None, None] + second[0] * right[..., None, None]  14.8 us
    all_to_all x1, starting transfers between devices, local(): lax.all_to_all(values3.reshape(seqs * pieces, sub, heads * vdim), 'sp', s...  10.2 us
    slice x4, local copies, waits for them, and re-layouts, merged(): tail = jax.tree.map(lambda part: part[1:], pieces)  6.89 us
    add x7, other arithmetic, merge_states(): normal = first[1] * left[..., None] + second[1] * right[..., None]  5.45 us
    unnamed x17, local copies, waits for them, and re-layouts  5.28 us
  transfers between devices with their start and end apart: 2, of which 0 were waited for; matrix products, arithmetic and copies ran while one was open for 3% of the time, Pallas kernels for 0%

commit v1 on v0

--- a/solution.py
+++ b/solution.py
@@ -69,12 +69,18 @@
     keys3 = keys.reshape(seqs, span, heads * kdim)
     values3 = values.reshape(seqs, span, heads * vdim)
     key_cache, value_cache = (
-        lax.all_to_all(
-            keys3.reshape(seqs * pieces, sub, heads * kdim),
-            "sp",
-            split_axis=0,
-            concat_axis=1,
-            tiled=True,
+        jnp.concatenate(
+            lax.all_to_all(
+                jnp.stack(
+                    jnp.split(
+                        keys3.reshape(seqs * pieces, sub, heads * kdim), lax.axis_size("sp"), axis=0
+                    )
+                ),
+                "sp",
+                0,
+                0,
+            ),
+            axis=1,
         ),
         lax.all_to_all(
             values3.reshape(seqs * pieces, sub, heads * vdim),

time: 213 us -> 252 us (1.18)
  other arithmetic: 40.9 us -> 61.9 us
  local copies, waits for them, and re-layouts: 24.3 us -> 40.5 us
    select_n x8, other arithmetic: 0.12 us -> 10.2 us  [step(): return jnp.where(reached, new, before)]
    another operation x3, other arithmetic: 4.93 us -> 11.3 us
    another operation x4 -> x5, local copies, waits for them, and re-layouts: 0.15 us -> 4.65 us
    reshape x2, local copies, waits for them, and re-layouts: 0.03 us -> 2.67 us
    slice x2, local copies, waits for them, and re-layouts: 0.21 us -> 2.84 us
    unnamed x17 -> x26, local copies, waits for them, and re-layouts: 5.28 us -> 5.9 us
  transfers between devices with their start and end apart: 2 -> 2, of which waited for: 0 -> 0; matrix products, arithmetic and copies ran while one was open for 3% -> 2% of each run, Pallas kernels for 0% -> 0%
where the time goes in v1:
time: 252 us; the launch traced here: 249 us
  blocking collectives  112 us (44%)
  other arithmetic  61.9 us (25%)
  local copies, waits for them, and re-layouts  40.5 us (16%)
  between operations  14.2 us (6%)
  matrix products  10.6 us (4%)
  starting transfers between devices  10.1 us (4%)
    all_gather x2, blocking collectives, merged(): pieces = jax.tree.map(lambda part: lax.all_gather(part, axis), value)  68.2 us
    all_gather x1, blocking collectives, carried_in(): everything = lax.all_gather(array, axis)  29 us
    add x7, other arithmetic, merge_states(): first[0] * left[..., None, None] + second[0] * right[..., None, None]  14.8 us
    all_to_all x1, blocking collectives, local(): lax.all_to_all(jnp.stack(jnp.split(keys3.reshape(seqs * pieces, sub, head...  14.6 us
    another operation x3, other arithmetic  11.3 us
    select_n x8, other arithmetic, step(): return jnp.where(reached, new, before)  10.2 us
    all_to_all x1, starting transfers between devices, local(): lax.all_to_all(values3.reshape(seqs * pieces, sub, heads * vdim), 'sp', s...  10.1 us
    slice x4, local copies, waits for them, and re-layouts, merged(): tail = jax.tree.map(lambda part: part[1:], pieces)  6.89 us
  transfers between devices with their start and end apart: 2, of which 0 were waited for; matrix products, arithmetic and copies ran while one was open for 2% of the time, Pallas kernels for 0%

profile of v1, /device:TPU:0, one launch (start us, length us, event | category | flops | bytes accessed | tf_op | source)
XLA Modules:
  0.0 249.2 jit_solution(16829823045683528822)
XLA Ops:
  7.2 1.8 copy-done
  9.1 2.4 convolution_convert_fusion.1
  11.4 2.7 %convolution_convert_fusion = bf16[768,512]{1,0:T(8,128)(2,1)} fusion(bf16[768,2048]{1,0:T(8,128)(2,1)S(1)} %bitcast.102, bf16[2048,512]{1,0:T(8,128)(2,1)S(1)} %copy-done.7), kind=kOutput, calls=%fused_computation.10 | convolution fusion | flops 1611005952 | bytes 6029312 | tf_op jit(solution)/shard_map/dot_general | solution.py:64
  14.1 1.1 copy.31
  15.2 2.8 %reshape.87 = f32[4,192,4,64]{1,0,3,2:T(4,128)} reshape(f32[768,256]{0,1:T(8,128)} %copy.31) | data formatting | bytes 1572864 | tf_op jit(solution)/shard_map/convert_element_type | solution.py:39
  18.1 1.6 convolution_bitcast_fusion
  20.4 0.8 reshape.83
  21.2 1.4 reshape.80
  22.6 1.4 reduce_sum.27
  24.0 1.3 pad.3
  25.3 1.3 reshape.81
  26.7 1.3 copy.34
  28.0 9.2 %reduce-window.6 = f32[4,4,2,128]{3,2,1,0:T(2,128)} reduce-window(f32[4,4,2,128]{3,2,1,0:T(2,128)} %copy.34, f32[]{:T(128)} %constant.71.clone.1), window={size=1x1x1x128 pad=0_0x0_0x0_0x127_0}, to_apply=%region_3.4 | reduce-window | flops 520192 | bytes 32772 | tf_op jit(solution)/shard_map/reduce-window
  37.2 1.4 slice.73
  38.6 1.4 copy.35
  41.3 1.4 copy.36
  42.7 1.4 broadcast_add_fusion
  44.1 1.3 reduce_window_sum.16
  45.4 1.3 copy.51
  46.8 1.3 copy.32
  48.1 29.0 %all-gather.4 = f32[8,4,4]{2,1,0:T(4,128)} all-gather(f32[1,4,4]{2,1,0:T(4,128)} %bitcast.113), channel_id=2, replica_groups=mesh['gr'=2,'sp'=8,'tp'=2] {'sp'}, dimensions={0}, use_global_device_ids=true | all-gather | bytes 576 | tf_op jit(solution)/shard_map/all_gather | solution.py:9
  77.1 10.2 %while.33 = (s32[]{:T(128)}, f32[4,4]{1,0:T(4,128)}, s32[]{:T(128)}, f32[8,4,4]{2,1,0:T(4,128)}, s32[]{:T(128)}, /*index=5*/s32[]{:T(128)}, s32[]{:T(128)}, s32[]{:T(128)}) while((s32[]{:T(128)}, f32[4,4]{1,0:T(4,128)}, s32[]{:T(128)}, f32[8,4,4]{2,1,0:T(4,128)}, s32[]{:T(128)}, /*index=5*/s32[]{:T(128)}, s32[]{:T(128)}, ...), condition=%wide.region_2.3_spmd.clone, body=%wide.region_1.2_spmd.clone.sunk | while | flops 56 | bytes 355 | solution.py:18
  77.1 1.3 add_select_fusion.2
  78.3 1.3 add_select_fusion.2
  79.6 1.3 add_select_fusion.2
  80.9 1.3 add_select_fusion.2
  82.1 1.3 add_select_fusion.2
  83.4 1.3 add_select_fusion.2
  84.7 1.3 add_select_fusion.2
  85.9 1.3 add_select_fusion.2
  87.2 1.3 copy.33
  89.2 0.9 fusion.22
  90.7 1.4 exponential_multiply_fusion
  92.1 2.4 reshape_reshape.9
  94.5 2.3 fusion.24
  96.8 2.9 %fusion.3 = f32[4,4,64,128]{3,2,1,0:T(8,128)} fusion(f32[4,192,4,64]{1,0,3,2:T(4,128)S(1)} %get-tuple-element.219, bf16[4,192,4,128]{3,2,1,0:T(4,128)(2,1)} %reshape_reshape.9), kind=kOutput, calls=%fused_computation.13 | convolution fusion | flops 301989888 | bytes 2097152 | tf_op jit(solution)/shard_map/slhd,slhe->shde/dot_general | solution.py:42
  99.9 14.6 %all_to_all.17 = bf16[8,1,96,256]{3,2,1,0:T(8,128)(2,1)S(1)} all-to-all(bf16[8,1,96,256]{3,2,1,0:T(8,128)(2,1)S(1)} %fusion.6), channel_id=1, replica_groups=mesh['gr'=2,'sp'=8,'tp'=2] {'sp'}, dimensions={0} | all-to-all | bytes 786432 | tf_op jit(solution)/shard_map/all_to_all | solution.py:73
  114.5 10.1 %all-to-all-start.1 = ((bf16[8,96,512]{2,1,0:T(8,128)(2,1)}), bf16[8,96,512]{2,1,0:T(8,128)(2,1)}, u32[]{:S(2)}, u32[]{:S(2)}) async-start(bf16[8,96,512]{2,1,0:T(8,128)(2,1)} %bitcast.105), calls=%async_computation.1 | async-start | bytes 1572864 | tf_op jit(solution)/shard_map/all_to_all | solution.py:85
  124.7 1.0 copy.40
  125.7 41.7 %all-gather.2 = f32[32,4,64]{2,1,0:T(4,128)S(1)} all-gather(f32[4,4,64]{2,1,0:T(4,128)S(1)} %copy.40), channel_id=4, replica_groups=mesh['gr'=2,'sp'=8,'tp'=2] {'sp'}, dimensions={0}, use_global_device_ids=true | all-gather | bytes 36864 | tf_op jit(solution)/shard_map/all_gather | solution.py:22
  168.0 1.3 slice.84
  170.7 26.5 %all-gather.5 = f32[8,4,4]{2,1,0:T(4,128)S(1)} all-gather(f32[1,4,4]{2,1,0:T(4,128)S(1)} %bitcast.112), channel_id=5, replica_groups=mesh['gr'=2,'sp'=8,'tp'=2] {'sp'}, dimensions={0}, use_global_device_ids=true | all-gather | bytes 576 | tf_op jit(solution)/shard_map/all_gather | solution.py:22
  198.5 1.9 slice.77
  200.3 4.4 %slice.82 = f32[28,4,64,128]{3,2,1,0:T(8,128)} slice(f32[32,4,64,128]{3,2,1,0:T(8,128)} %all-gather.8.cloned.1.call-done), slice={[4:32], [0:4], [0:64], [0:128]} | slice | bytes 7340032 | tf_op jit(solution)/shard_map/slice | solution.py:24
  204.7 30.0 %while.32 = (s32[]{:T(128)}, f32[4,4,64,128]{3,2,1,0:T(8,128)}, f32[4,4,64]{2,1,0:T(4,128)S(1)}, f32[4,4]{1,0:T(4,128)S(1)}, f32[4,4]{1,0:T(4,128)S(1)}, /*index...) while((s32[]{:T(128)}, f32[4,4,64,128]{3,2,1,0:T(8,128)}, ...), condition=%wide.region_8.9_spmd, body=%wide.region_7.8_spmd.sunk | while | flops 396354 | bytes 1586173 | solution.py:25
  206.1 2.1 fusion.35
  208.2 0.8 fusion.36
  210.4 2.1 fusion.35
  212.5 0.8 fusion.36
  214.6 2.1 fusion.35
  216.8 0.8 fusion.36
  218.9 2.1 fusion.35
  221.0 0.8 fusion.36
  223.2 2.1 fusion.35
  225.3 0.8 fusion.36
  227.5 2.1 fusion.35
  229.6 0.8 fusion.36
  231.8 2.1 fusion.35
  233.9 0.8 fusion.36
  235.3 1.1 broadcast_multiply_fusion.1
  236.5 1.4 multiply_reduce_fusion
  237.8 1.0 fusion.25
  239.6 0.7 copy.85
  240.3 2.1 copy.86
  (58 shorter events, 17.7 us)
Async XLA Ops:
  7.2 1.9 copy-start
  7.2 191.3 %all-gather.8.cloned.1.call-start = ((), (), s32[]{:S(2)}) async-start(), calls=%async_computation.2 | async-start | bytes 4718592 | tf_op jit(solution)/shard_map/all_gather | solution.py:22
  9.1 2.4 copy-start.7
  11.4 6.6 %copy-start.4 = (bf16[2048,4]{0,1:T(4,128)(2,1)S(1)}, bf16[2048,4]{0,1:T(4,128)(2,1)}, u32[]{:S(2)}) copy-start(bf16[2048,4]{0,1:T(4,128)(2,1)} %param.15) | copy-start | bytes 49156
  18.1 1.6 copy-start.6
  90.1 0.6 copy-start.2
  96.8 27.7 %copy-start.3 = (f32[4,4]{0,1:T(4,128)S(1)}, f32[4,4]{0,1:T(4,128)}, u32[]{:S(2)}) copy-start(f32[4,4]{0,1:T(4,128)} %copy-done.2) | copy-start | bytes 196
  96.8 72.5 %copy-start.5 = (bf16[4,256]{1,0:T(4,128)(2,1)S(1)}, bf16[4,256]{1,0:T(4,128)(2,1)}, u32[]{:S(2)}) copy-start(bf16[4,256]{1,0:T(4,128)(2,1)} %param.17) | copy-start | bytes 6148
  114.5 84.0 %all-to-all-start.1 = ((bf16[8,96,512]{2,1,0:T(8,128)(2,1)}), bf16[8,96,512]{2,1,0:T(8,128)(2,1)}, u32[]{:S(2)}, u32[]{:S(2)}) async-start(bf16[8,96,512]{2,1,0:T(8,128)(2,1)} %bitcast.105), calls=%async_computation.1 | async-start | bytes 1572864 | tf_op jit(solution)/shard_map/all_to_all | solution.py:85
  236.5 5.9 %copy-start.1 = (f32[4,4,64,128]{3,2,1,0:T(8,128)}, f32[4,4,64,128]{3,2,1,0:T(8,128)S(1)}, u32[]{:S(2)}) copy-start(f32[4,4,64,128]{3,2,1,0:T(8,128)S(1)} %broadcast_multiply_fusion.1) | copy-start | bytes 1572868
Sparse Core Ops, SparseCore 0:
  99.9 87.7 all-gather.7
